TPU v7x, 32 devices: a whole 2x2x4 slice. The times are simulated.
32 devices in a mesh: dp: 4 (over y, x), kv: 4 (over z), tp: 2 (over core).
Axes of the slice: x: 2, y: 2, z: 4, core: 2. Of those that a mesh axis runs over, the one named last changes fastest.
Arguments:
- tokens: bfloat16 [32, 2048], P('dp', 'kv'), may hold values from -6 to 6
- pre_gain: float32 [2048], P('kv'), may hold values from 0.1 to 1.9
- query_weight: bfloat16 [2048, 1024], P('kv', 'tp'), may hold values from -0.125 to 0.125
- key_weight: bfloat16 [2048, 1024], P('kv', 'tp'), may hold values from -0.125 to 0.125
- value_weight: bfloat16 [2048, 1024], P('kv', 'tp'), may hold values from -0.125 to 0.125
- outgate_weight: bfloat16 [2048, 1024], P('kv', 'tp'), may hold values from -0.125 to 0.125
- input_gate_weight: bfloat16 [2048, 4], replicated, may hold values from -0.125 to 0.125
- forget_gate_weight: bfloat16 [2048, 4], replicated, may hold values from -0.125 to 0.125
- cache_keys: bfloat16 [32, 64, 1024], P(('dp', 'kv'), None, 'tp'), may hold values from -6 to 6
- cache_values: bfloat16 [32, 64, 1024], P(('dp', 'kv'), None, 'tp'), may hold values from -6 to 6
- cache_input: float32 [32, 64, 4], P(('dp', 'kv'), None, 'tp'), may hold values from -6 to 250
- cache_forget: float32 [32, 64, 4], P(('dp', 'kv'), None, 'tp'), may hold values from -0.7 to 0
- lengths: int32 [32], P(('dp', 'kv')), may hold values from 1 to 64, 819 in all
- state_matrix: float32 [32, 4, 256, 256], P(('dp', 'kv'), 'tp'), may hold values from -6 to 6
- state_norm: float32 [32, 4, 256], P(('dp', 'kv'), 'tp'), may hold values from -6 to 6
- state_max: float32 [32, 4], P(('dp', 'kv'), 'tp'), may hold values from -4 to 253
- head_gain: float32 [1024], P('tp'), may hold values from 0.1 to 1.9
- out_weight: bfloat16 [1024, 2048], P('tp', 'kv'), may hold values from -0.375 to 0.375
- mixer_gain: float32 [2048], replicated, may hold values from 0.1 to 1.9
- gate_weight: bfloat16 [2048, 5632], P(None, ('kv', 'tp')), may hold values from -0.125 to 0.125
- up_weight: bfloat16 [2048, 5632], P(None, ('kv', 'tp')), may hold values from -0.125 to 0.125
- down_weight: bfloat16 [5632, 2048], P(('kv', 'tp')), may hold values from -0.21875 to 0.21875
Outputs:
- layer_out: bfloat16 [32, 2048], P('dp', ('kv', 'tp'))
Inputs may be any that keep to these rules, and one draw needn't show every extreme that they name: `lengths`: positions from a sequence's length on take no part.
All inputs are finite; a program needn't handle non-finite values. No bound on the sum of `lengths` on one device may be relied on, other than what follows from the above.
Results may differ from a plain program's by a relative error of at most 0.018.
Values may be sent and summed in bfloat16 or wider, within the bound.
No kernel may reach another device: no remote copies, remote signals or barrier semaphores. Data moves between devices by JAX's collectives and lax.ppermute only.
A program may use at most 64 MiB of HBM per device.

v0:
```python
import jax
import jax.numpy as jnp
from jax import lax
from jax.sharding import PartitionSpec as P

EPS = 1e-06


def per_device(
    tokens,
    pre_gain,
    query_weight,
    key_weight,
    value_weight,
    outgate_weight,
    input_gate_weight,
    forget_gate_weight,
    cache_keys,
    cache_values,
    cache_input,
    cache_forget,
    lengths,
    state_matrix,
    state_norm,
    state_max,
    head_gain,
    out_weight,
    mixer_gain,
    gate_weight,
    up_weight,
    down_weight,
):
    col_width = tokens.shape[1]
    own_seqs = cache_keys.shape[0]
    block_len = cache_keys.shape[1]
    head_count = state_max.shape[1]
    head_size = state_norm.shape[2]
    shard_index = lax.axis_index("kv")
    half_index = lax.axis_index("tp")
    kv_count = lax.axis_size("kv")
    model_width = col_width * kv_count
    token_values = tokens.astype(jnp.float32)
    squares = jnp.sum(token_values * token_values, axis=1)
    normed = (token_values * pre_gain[None, :]).astype(jnp.bfloat16)
    corner = (shard_index * col_width, half_index * head_count)
    gate_pair = jnp.concatenate(
        [
            lax.dynamic_slice(input_gate_weight, corner, (col_width, head_count)),
            lax.dynamic_slice(forget_gate_weight, corner, (col_width, head_count)),
        ],
        axis=1,
    )

    def product(weight):
        return jnp.dot(normed, weight, preferred_element_type=jnp.float32)

    query_term = product(query_weight)
    key_term = product(key_weight)
    value_term = product(value_weight)
    outgate_term = product(outgate_weight)
    gate_term = product(gate_pair)
    square_totals = lax.psum(squares, "kv")
    query_sum, key_sum, value_sum, outgate_sum, gate_sum = (
        lax.psum_scatter(query_term, "kv", scatter_dimension=0, tiled=True),
        lax.psum_scatter(key_term, "kv", scatter_dimension=0, tiled=True),
        lax.psum_scatter(value_term, "kv", scatter_dimension=0, tiled=True),
        lax.psum_scatter(outgate_term, "kv", scatter_dimension=0, tiled=True),
        lax.psum_scatter(gate_term, "kv", scatter_dimension=0, tiled=True),
    )
    own_squares = lax.dynamic_slice_in_dim(square_totals, shard_index * own_seqs, own_seqs, 0)
    scale_first = lax.rsqrt(own_squares / model_width + EPS)[:, None]
    query = (scale_first * query_sum).astype(jnp.bfloat16)
    keys_new = (scale_first * key_sum).astype(jnp.bfloat16)
    values_new = (scale_first * value_sum).astype(jnp.bfloat16)
    outgate = (scale_first * outgate_sum).astype(jnp.bfloat16)
    gate_values = scale_first * gate_sum
    in_gate = gate_values[:, :head_count]
    forget_new = jax.nn.log_sigmoid(gate_values[:, head_count:])
    query_heads = query.reshape(own_seqs, head_count, head_size)
    key_heads = keys_new.reshape(own_seqs, head_count, head_size)
    value_heads = values_new.reshape(own_seqs, head_count, head_size)
    cached_keys = cache_keys.reshape(own_seqs, block_len, head_count, head_size)
    cached_values = cache_values.reshape(own_seqs, block_len, head_count, head_size)
    inv_root = head_size ** (-0.5)
    live_mask = (lax.broadcasted_iota(jnp.int32, (own_seqs, block_len), 1) < lengths[:, None])[
        :, :, None
    ]
    forget_live = jnp.where(live_mask, cache_forget, jnp.float32(0.0))
    running = jnp.cumsum(forget_live, axis=1)
    total_log = running[:, -1, :] + forget_new
    weight_log = jnp.where(live_mask, total_log[:, None, :] - running + cache_input, -jnp.inf)
    state_log = total_log + state_max
    peak_log = jnp.maximum(jnp.maximum(state_log, in_gate), jnp.max(weight_log, axis=1))
    key_dots = (
        jnp.einsum("shd,slhd->slh", query_heads, cached_keys, preferred_element_type=jnp.float32)
        * inv_root
    )
    block_scores = jnp.exp(weight_log - peak_log[:, None, :]) * key_dots
    query_scaled = query_heads.astype(jnp.float32) * inv_root
    self_score = jnp.exp(in_gate - peak_log) * jnp.sum(
        query_scaled * key_heads.astype(jnp.float32), axis=2
    )
    carried = jnp.exp(state_log - peak_log)
    block_weights = block_scores.astype(jnp.bfloat16)
    memory_read = jnp.einsum(
        "shvd,shd->shv", state_matrix, query_scaled, precision=lax.Precision.HIGHEST
    )
    norm_read = jnp.einsum("shd,shd->sh", state_norm, query_scaled, precision=lax.Precision.HIGHEST)
    numerator = (
        carried[:, :, None] * memory_read
        + jnp.einsum(
            "slh,slhd->shd", block_weights, cached_values, preferred_element_type=jnp.float32
        )
        + self_score[:, :, None] * value_heads.astype(jnp.float32)
    )
    denominator = carried * norm_read + jnp.sum(block_scores, axis=1) + self_score
    hidden = numerator / jnp.maximum(jnp.abs(denominator), 1.0)[:, :, None]
    mixed_heads = (
        hidden.reshape(own_seqs, head_count * head_size)
        * head_gain[None, :]
        * jax.nn.sigmoid(outgate.astype(jnp.float32))
    ).astype(jnp.bfloat16)
    mix_terms = jnp.dot(
        lax.all_gather(mixed_heads, "kv", axis=0, tiled=True),
        out_weight,
        preferred_element_type=jnp.float32,
    )
    mix_sum = lax.psum_scatter(
        mix_terms.astype(jnp.bfloat16), "tp", scatter_dimension=1, tiled=True
    ).astype(jnp.float32)
    narrow = mix_sum.shape[1]
    residual = (
        lax.dynamic_slice_in_dim(token_values, half_index * narrow, narrow, 1) + mix_sum
    ).astype(jnp.bfloat16)
    piece_wide = lax.all_gather(residual, ("kv", "tp"), axis=1, tiled=True).astype(jnp.float32)
    normed_piece = (piece_wide * mixer_gain[None, :]).astype(jnp.bfloat16)
    gate_acc = jnp.dot(normed_piece, gate_weight, preferred_element_type=jnp.float32)
    up_acc = jnp.dot(normed_piece, up_weight, preferred_element_type=jnp.float32)
    sum_squares = jnp.sum(piece_wide * piece_wide, axis=1)
    gate_acc, up_acc, sum_squares = (gate_acc, up_acc, sum_squares)
    scale_mid = lax.rsqrt(sum_squares / model_width + EPS)[:, None]
    hidden_units = (jax.nn.silu(scale_mid * gate_acc) * (scale_mid * up_acc)).astype(jnp.bfloat16)
    summed = lax.psum_scatter(
        lax.dot_general(
            down_weight, hidden_units, (((0,), (1,)), ((), ())), preferred_element_type=jnp.float32
        ),
        ("kv", "tp"),
        scatter_dimension=0,
        tiled=True,
    )
    mixer_out = summed.T
    return (residual.astype(jnp.float32) + mixer_out).astype(jnp.bfloat16)


def solution(mesh):
    in_specs = (
        P("dp", "kv"),
        P("kv"),
        P("kv", "tp"),
        P("kv", "tp"),
        P("kv", "tp"),
        P("kv", "tp"),
        P(),
        P(),
        P(("dp", "kv"), None, "tp"),
        P(("dp", "kv"), None, "tp"),
        P(("dp", "kv"), None, "tp"),
        P(("dp", "kv"), None, "tp"),
        P(("dp", "kv")),
        P(("dp", "kv"), "tp", None, None),
        P(("dp", "kv"), "tp", None),
        P(("dp", "kv"), "tp"),
        P("tp"),
        P("tp", "kv"),
        P(),
        P(None, ("kv", "tp")),
        P(None, ("kv", "tp")),
        P(("kv", "tp"), None),
    )
    out_specs = P("dp", ("kv", "tp"))
    return jax.shard_map(
        per_device, mesh=mesh, in_specs=in_specs, out_specs=out_specs, check_vma=False
    )
```

profile of v0, /device:TPU:0, one launch (start us, length us, event | category | flops | bytes accessed | tf_op | source)
XLA Modules:
  0.0 147.6 jit_solution(3637259032463186697)
XLA Ops:
  6.5 0.0 copy-start
  6.5 0.0 all-reduce.8.cloned.1.call-start
  6.6 1.6 %multiply_reduce_fusion = f32[8]{0:T(128)} fusion(bf16[8,512]{1,0:T(8,128)(2,1)} %param.22), kind=kLoop, calls=%fused_computation.22 | loop fusion | flops 12280 | bytes 8224 | tf_op jit(solution)/shard_map/reduce_sum | solution.py:43
  8.2 1.9 %fusion.43 = f32[8,512]{1,0:T(8,128)} fusion(bf16[512,512]{1,0:T(8,128)(2,1)} %param.27, f32[512]{0:T(512)} %param.23, bf16[8,512]{1,0:T(8,128)(2,1)} %param.22), kind=kOutput, calls=%fused_computation.73 | convolution fusion | flops 4206592 | bytes 550912 | tf_op jit(solution)/shard_map/dot_general | solution.py:55
  10.0 1.9 %fusion.44 = f32[8,512]{1,0:T(8,128)} fusion(bf16[512,512]{1,0:T(8,128)(2,1)} %param.26, f32[512]{0:T(512)} %param.23, bf16[8,512]{1,0:T(8,128)(2,1)} %param.22), kind=kOutput, calls=%fused_computation.74 | convolution fusion | flops 4206592 | bytes 550912 | tf_op jit(solution)/shard_map/dot_general | solution.py:55
  11.9 1.9 %fusion.46 = f32[8,512]{1,0:T(8,128)} fusion(bf16[512,512]{1,0:T(8,128)(2,1)} %param.24, f32[512]{0:T(512)} %param.23, bf16[8,512]{1,0:T(8,128)(2,1)} %param.22), kind=kOutput, calls=%fused_computation.76 | convolution fusion | flops 4206592 | bytes 550912 | tf_op jit(solution)/shard_map/dot_general | solution.py:55
  13.7 0.8 dynamic_slice.15
  14.5 0.8 dynamic_slice.14
  15.3 1.9 %fusion.45 = f32[8,512]{1,0:T(8,128)} fusion(bf16[512,512]{1,0:T(8,128)(2,1)} %param.25, f32[512]{0:T(512)} %param.23, bf16[8,512]{1,0:T(8,128)(2,1)} %param.22), kind=kOutput, calls=%fused_computation.75 | convolution fusion | flops 4206592 | bytes 550912 | tf_op jit(solution)/shard_map/dot_general | solution.py:55
  17.1 1.4 fusion.21
  18.5 0.0 all-reduce.8.cloned.1.call-update
  18.6 0.0 reduce-scatter.3.cloned.1.call-start
  18.6 0.7 iota_compare_fusion
  19.3 0.7 broadcast_select_fusion
  20.0 0.0 copy-done.4
  20.0 0.1 copy.39
  20.1 0.1 reduce_window_sum.11
  20.2 0.1 copy.40
  20.3 1.3 dynamic-slice
  22.3 34.1 %all-reduce.8.cloned.1.call-done = (f32[8,512]{1,0:T(8,128)}, f32[8]{0:T(128)}, f32[8,512]{1,0:T(8,128)}, f32[8,512]{1,0:T(8,128)}, f32[8,4]{1,0:T(8,128)}, /*index=5*/f32[8,512]{1,0:T(8,128)}) async-done(((f32[8,512]{1,0:T(8,128)}, f32[8]{0:T(128)}, f32[8,512]{1,0:T(8,128)}, f32[8,512]{1,0:T(8,128)}, f32[8,4]{1,0:T(8,128)}, /*index=5*/f32[8,512]{1,0:T(8,128)}), (f32[8,512]{1,0:T(8,128)}, f32[8]{0:T(128)}, ...) | async-done | bytes 65712
  56.3 0.7 add_rsqrt_fusion.1
  57.1 0.8 fusion.37
  57.9 0.7 fusion.40
  58.7 1.0 fusion.5
  59.7 0.1 fusion.42
  59.8 0.9 fusion.49
  60.7 0.7 maximum_maximum_fusion
  61.4 0.8 fusion.50
  62.2 1.0 fusion.2
  63.2 0.8 multiply_reduce_fusion.1
  64.0 2.2 %fusion.31 = f32[2,2,1,256]{3,2,1,0:T(1,128)S(1)} fusion(f32[2,2,256,256]{3,2,1,0:T(8,128)} %param.35, f32[2,2,256,1]{2,1,0,3:T(2,128)S(1)} %get-tuple-element.20), kind=kOutput, calls=%fused_computation.46 | convolution fusion | flops 3145728 | bytes 1056768 | tf_op jit(solution)/shard_map/shvd,shd->shv/dot_general | solution.py:105
  66.2 0.1 fusion.35
  66.3 0.8 fusion.39
  67.1 12.0 %all-gather = bf16[4,2,512]{2,1,0:T(2,128)(2,1)S(1)} all-gather(bf16[1,2,512]{2,1,0:T(2,128)(2,1)S(1)} %fusion.39), channel_id=1, replica_groups=mesh['dp'=4,'kv'=4,'tp'=2] {'kv'}, dimensions={0}, use_global_device_ids=true | all-gather | bytes 10240 | tf_op jit(solution)/shard_map/all_gather | solution.py:124
  79.1 0.8 convolution_convert_fusion
  79.9 0.0 reduce-scatter.3.cloned.1.call-update
  79.9 0.0 reduce-scatter.5.cloned.1.call-start
  80.0 0.0 copy-done.2
  80.0 6.4 %reduce-scatter.3.cloned.1.call-done = bf16[8,256]{1,0:T(8,128)(2,1)} async-done(((bf16[8,512]{1,0:T(8,128)(2,1)}), bf16[8,256]{1,0:T(8,128)(2,1)}) %reduce-scatter.3.cloned.1.call-update) | async-done | bytes 4112 | tf_op jit(solution)/shard_map/reduce_scatter | solution.py:128
  86.3 0.7 add_convert_fusion
  87.0 14.3 %all_gather.7 = bf16[8,2048]{1,0:T(8,128)(2,1)S(1)} all-gather(bf16[8,256]{1,0:T(8,128)(2,1)S(1)} %add_convert_fusion), channel_id=1, replica_groups=mesh['dp'=4,'kv'=4,'tp'=2] {'kv','tp'}, dimensions={1}, use_global_device_ids=true | all-gather | bytes 36864 | tf_op jit(solution)/shard_map/all_gather | solution.py:135
  101.3 0.1 fusion.8
  101.5 2.7 %convolution_multiply_fusion.1 = f32[8,704]{1,0:T(8,128)S(1)} fusion(bf16[2048,704]{0,1:T(8,128)(2,1)} %param.41, bf16[8,2048]{1,0:T(8,128)(2,1)S(1)} %all_gather.7, f32[2048]{0:T(1024)S(1)} %copy-done.3, f32[8]{0:T(128)S(1)} %add_rsqrt_fusion), kind=kOutput, calls=%fused_computation.3 | convolution fusion | flops 23123456 | bytes 2947104 | tf_op jit(solution)/shard_map/dot_general | solution.py:137
  104.2 0.0 copy-done
  104.2 4.1 %convolution_bitcast_fusion = f32[2048,8]{0,1:T(8,128)} fusion(bf16[704,2048]{1,0:T(8,128)(2,1)S(1)} %copy-done, bf16[2048,704]{0,1:T(8,128)(2,1)} %param.42, bf16[8,2048]{1,0:T(8,128)(2,1)S(1)} %all_gather.7, f32[2048]{0:T(1024)S(1)} %copy-done.3, f32[8,704]{1,0:T(8,128)S(1)} %convolution_multiply_fusion.1, f32[8]{0:T(128)S(1)} %add_rsqrt_fusion), kind=kOutput, calls=%fused_computation | convolution fusion | flops 46225920 | bytes 5896224 | tf_op jit(solution)/shard_map/dot_general | solution.py:144
  108.3 0.0 reduce-scatter.5.cloned.1.call-update
  108.3 31.5 %reduce-scatter.5.cloned.1.call-done = f32[256,8]{0,1:T(8,128)} async-done(((f32[2048,8]{0,1:T(8,128)}), f32[256,8]{0,1:T(8,128)}) %reduce-scatter.5.cloned.1.call-update) | async-done | bytes 8208 | tf_op jit(solution)/shard_map/reduce_scatter | solution.py:143
  139.8 1.3 fusion.20
  (16 shorter events, 0.1 us)
Async XLA Ops:
  6.5 97.6 %copy-start = (bf16[704,2048]{1,0:T(8,128)(2,1)S(1)}, bf16[704,2048]{1,0:T(8,128)(2,1)}, u32[]{:S(2)}) copy-start(bf16[704,2048]{1,0:T(8,128)(2,1)} %param.43) | copy-start | bytes 8650756
  6.5 73.4 %copy-start.2 = (bf16[8,512]{1,0:T(8,128)(2,1)S(1)}, bf16[8,512]{1,0:T(8,128)(2,1)}, u32[]{:S(2)}) copy-start(bf16[8,512]{1,0:T(8,128)(2,1)} %param.22) | copy-start | bytes 24580
  6.5 72.6 %copy-start.1 = (bf16[512,512]{1,0:T(8,128)(2,1)S(1)}, bf16[512,512]{1,0:T(8,128)(2,1)}, u32[]{:S(2)}) copy-start(bf16[512,512]{1,0:T(8,128)(2,1)} %param.39) | copy-start | bytes 1572868
  6.5 94.9 %copy-start.3 = (f32[2048]{0:T(1024)S(1)}, f32[2048]{0:T(1024)}, u32[]{:S(2)}) copy-start(f32[2048]{0:T(1024)} %param.40) | copy-start | bytes 24580
  6.5 49.8 %all-reduce.8.cloned.1.call-start = ((), (), s32[]{:S(2)}) async-start(), calls=%async_computation.4 | async-start | bytes 140288
  18.6 67.8 %reduce-scatter.3.cloned.1.call-start = ((), (), s32[]{:S(2)}) async-start(), calls=%async_computation.2 | async-start | bytes 12288 | tf_op jit(solution)/shard_map/reduce_scatter | solution.py:128
  19.3 0.7 copy-start.4
  79.9 59.9 %reduce-scatter.5.cloned.1.call-start = ((), (), s32[]{:S(2)}) async-start(), calls=%async_computation.3 | async-start | bytes 73728 | tf_op jit(solution)/shard_map/reduce_scatter | solution.py:143
Sparse Core Ops, SparseCore 0:
  18.7 37.6 all-reduce.7
  80.0 6.2 reduce-scatter.2
  108.4 31.2 reduce-scatter.4
where the time goes:
time: 149 us; the launch traced here: 148 us
  waiting for transfers between devices  71.9 us (48%)
  blocking collectives  26.3 us (18%)
  matrix products  20.6 us (14%)
  between operations  13.8 us (9%)
  other arithmetic  11.7 us (8%)
  local copies, waits for them, and re-layouts  3.11 us (2%)
    unnamed x4, waiting for transfers between devices  34.1 us
    reduce_scatter x1, waiting for transfers between devices, per_device(): lax.psum_scatter(lax.dot_general(down_weight, hidden_units, (((0,), (1,))...  31.5 us
    all_gather x1, blocking collectives, per_device(): lax.all_gather(residual, ('kv', 'tp'), axis=1, tiled=True)  14.3 us
    all_gather x1, blocking collectives, per_device(): lax.all_gather(mixed_heads, 'kv', axis=0, tiled=True)  12 us
    dot_general x5, matrix products, product(): return jnp.dot(normed, weight, preferred_element_type=jnp.float32)  8.84 us
    reduce_scatter x1, waiting for transfers between devices, per_device(): lax.psum_scatter(mix_terms.astype(jnp.bfloat16), 'tp', scatter_dimension=...  6.35 us
    dot_general x1, matrix products, per_device(): lax.dot_general(down_weight, hidden_units, (((0,), (1,)), ((), ())), pref...  4.12 us
  transfers between devices with their start and end apart: 3, of which 3 were waited for; matrix products, arithmetic and copies ran while one was open for 2% of the time, Pallas kernels for 0%

commit v1 on v0

--- a/solution.py
+++ b/solution.py
@@ -4,6 +4,18 @@
 from jax.sharding import PartitionSpec as P
 
 EPS = 1e-06
+
+
+def collect(array, axis, dim):
+    ways, here = (lax.axis_size(axis), lax.axis_index(axis))
+    grown, reach = (array, 1)
+    while reach < ways:
+        theirs = lax.ppermute(grown, axis, [(d, d ^ reach) for d in range(ways)])
+        mine_first = jnp.concatenate([grown, theirs], axis=dim)
+        theirs_first = jnp.concatenate([theirs, grown], axis=dim)
+        grown = jnp.where(here & reach == 0, mine_first, theirs_first)
+        reach = 2 * reach
+    return grown
 
 
 def per_device(
@@ -121,9 +133,7 @@
         * jax.nn.sigmoid(outgate.astype(jnp.float32))
     ).astype(jnp.bfloat16)
     mix_terms = jnp.dot(
-        lax.all_gather(mixed_heads, "kv", axis=0, tiled=True),
-        out_weight,
-        preferred_element_type=jnp.float32,
+        collect(mixed_heads, "kv", 0), out_weight, preferred_element_type=jnp.float32
     )
     mix_sum = lax.psum_scatter(
         mix_terms.astype(jnp.bfloat16), "tp", scatter_dimension=1, tiled=True

time: 149 us -> 146 us (0.980)
  blocking collectives: 26.3 us -> 14.3 us
  waiting for transfers between devices: 71.9 us -> 77.5 us
  starting transfers between devices: 0.12 us -> 4.21 us
    all_gather x1 -> x0, blocking collectives: 12 us -> none  [per_device(): lax.all_gather(mixed_heads, 'kv', axis=0, tiled=True)]
    ppermute x0 -> x2, waiting for transfers between devices: none -> 4.12 us  [collect(): theirs = lax.ppermute(grown, axis, [(d, d ^ reach) for d in range(ways)])]
    ppermute x0 -> x2, starting transfers between devices: none -> 4.1 us  [collect(): theirs = lax.ppermute(grown, axis, [(d, d ^ reach) for d in range(ways)])]
  transfers between devices with their start and end apart: 3 -> 5, of which waited for: 3 -> 5; matrix products, arithmetic and copies ran while one was open for 2% -> 2% of each run, Pallas kernels for 0% -> 0%
where the time goes in v1:
time: 146 us; the launch traced here: 145 us
  waiting for transfers between devices  77.5 us (53%)
  matrix products  20.6 us (14%)
  blocking collectives  14.3 us (10%)
  between operations  13.8 us (9%)
  other arithmetic  11.7 us (8%)
  starting transfers between devices  4.21 us (3%)
  local copies, waits for them, and re-layouts  3.1 us (2%)
    unnamed x4, waiting for transfers between devices  34.1 us
    reduce_scatter x1, waiting for transfers between devices, per_device(): lax.psum_scatter(lax.dot_general(down_weight, hidden_units, (((0,), (1,))...  31.5 us
    all_gather x1, blocking collectives, per_device(): lax.all_gather(residual, ('kv', 'tp'), axis=1, tiled=True)  14.3 us
    dot_general x5, matrix products, product(): return jnp.dot(normed, weight, preferred_element_type=jnp.float32)  8.84 us
    reduce_scatter x1, waiting for transfers between devices, per_device(): lax.psum_scatter(mix_terms.astype(jnp.bfloat16), 'tp', scatter_dimension=...  7.67 us
    ppermute x2, waiting for transfers between devices, collect(): theirs = lax.ppermute(grown, axis, [(d, d ^ reach) for d in range(ways)])  4.12 us
    dot_general x1, matrix products, per_device(): lax.dot_general(down_weight, hidden_units, (((0,), (1,)), ((), ())), pref...  4.12 us
    ppermute x2, starting transfers between devices, collect(): theirs = lax.ppermute(grown, axis, [(d, d ^ reach) for d in range(ways)])  4.1 us
  transfers between devices with their start and end apart: 5, of which 5 were waited for; matrix products, arithmetic and copies ran while one was open for 2% of the time, Pallas kernels for 0%

profile of v1, /device:TPU:0, one launch (start us, length us, event | category | flops | bytes accessed | tf_op | source)
XLA Modules:
  0.0 145.3 jit_solution(15174428867666934797)
XLA Ops:
  6.5 0.0 all-reduce.8.cloned.1.call-start
  6.6 1.6 %multiply_reduce_fusion = f32[8]{0:T(128)} fusion(bf16[8,512]{1,0:T(8,128)(2,1)} %param.22), kind=kLoop, calls=%fused_computation.22 | loop fusion | flops 12280 | bytes 8224 | tf_op jit(solution)/shard_map/reduce_sum | solution.py:55
  8.2 1.9 %fusion.49 = f32[8,512]{1,0:T(8,128)} fusion(bf16[512,512]{1,0:T(8,128)(2,1)} %param.26, f32[512]{0:T(512)} %param.23, bf16[8,512]{1,0:T(8,128)(2,1)} %param.22), kind=kOutput, calls=%fused_computation.81 | convolution fusion | flops 4206592 | bytes 550912 | tf_op jit(solution)/shard_map/dot_general | solution.py:67
  10.0 1.9 %fusion.51 = f32[8,512]{1,0:T(8,128)} fusion(bf16[512,512]{1,0:T(8,128)(2,1)} %param.24, f32[512]{0:T(512)} %param.23, bf16[8,512]{1,0:T(8,128)(2,1)} %param.22), kind=kOutput, calls=%fused_computation.83 | convolution fusion | flops 4206592 | bytes 550912 | tf_op jit(solution)/shard_map/dot_general | solution.py:67
  11.9 0.8 dynamic_slice.15
  12.6 0.8 dynamic_slice.14
  13.4 1.9 %fusion.50 = f32[8,512]{1,0:T(8,128)} fusion(bf16[512,512]{1,0:T(8,128)(2,1)} %param.25, f32[512]{0:T(512)} %param.23, bf16[8,512]{1,0:T(8,128)(2,1)} %param.22), kind=kOutput, calls=%fused_computation.82 | convolution fusion | flops 4206592 | bytes 550912 | tf_op jit(solution)/shard_map/dot_general | solution.py:67
  15.3 1.9 %fusion.48 = f32[8,512]{1,0:T(8,128)} fusion(bf16[512,512]{1,0:T(8,128)(2,1)} %param.27, f32[512]{0:T(512)} %param.23, bf16[8,512]{1,0:T(8,128)(2,1)} %param.22), kind=kOutput, calls=%fused_computation.80 | convolution fusion | flops 4206592 | bytes 550912 | tf_op jit(solution)/shard_map/dot_general | solution.py:67
  17.1 1.4 fusion.27
  18.5 0.0 all-reduce.8.cloned.1.call-update
  18.6 0.0 reduce-scatter.3.cloned.1.call-start
  18.6 0.7 iota_compare_fusion
  19.3 0.7 broadcast_select_fusion
  20.0 0.1 copy.39
  20.1 0.1 reduce_window_sum.11
  20.2 0.1 copy.40
  20.3 1.3 dynamic-slice
  22.3 34.1 %all-reduce.8.cloned.1.call-done = (f32[8,512]{1,0:T(8,128)}, f32[8]{0:T(128)}, f32[8,512]{1,0:T(8,128)}, f32[8,4]{1,0:T(8,128)}, f32[8,512]{1,0:T(8,128)}, /*index=5*/f32[8,512]{1,0:T(8,128)}) async-done(((f32[8,512]{1,0:T(8,128)}, f32[8]{0:T(128)}, f32[8,512]{1,0:T(8,128)}, f32[8,4]{1,0:T(8,128)}, f32[8,512]{1,0:T(8,128)}, /*index=5*/f32[8,512]{1,0:T(8,128)}), (f32[8,512]{1,0:T(8,128)}, f32[8]{0:T(128)}, ...) | async-done | bytes 65712
  56.3 0.7 add_rsqrt_fusion.1
  57.1 0.8 fusion.43
  57.9 0.7 fusion.45
  58.7 1.0 fusion.5
  59.7 0.1 fusion.47
  59.8 0.9 fusion.55
  60.7 0.7 maximum_maximum_fusion
  61.4 0.8 fusion.56
  62.2 1.0 fusion.2
  63.3 0.8 multiply_reduce_fusion.1
  64.0 2.2 %fusion.37 = f32[2,2,1,256]{3,2,1,0:T(1,128)S(1)} fusion(f32[2,2,256,256]{3,2,1,0:T(8,128)} %param.35, f32[2,2,256,1]{2,1,0,3:T(2,128)S(1)} %get-tuple-element.20), kind=kOutput, calls=%fused_computation.54 | convolution fusion | flops 3145728 | bytes 1056768 | tf_op jit(solution)/shard_map/shvd,shd->shv/dot_general | solution.py:117
  66.2 0.1 fusion.41
  66.3 0.8 fusion.40
  67.1 1.6 %collective-permute-start = (bf16[2,512]{1,0:T(2,128)(2,1)S(1)}, bf16[2,512]{1,0:T(2,128)(2,1)S(1)}, u32[]{:S(2)}, u32[]{:S(2)}) collective-permute-start(bf16[2,512]{1,0:T(2,128)(2,1)S(1)} %fusion.40), channel_id=1, source_target_pairs={{0,2},{2,0},{4,6},{6,4},{1,3},{3,1},{5,7},{7,5},{8,10},{10,8},{12,... | collective-permute-start | bytes 6152 | tf_op jit(solution)/shard_map/ppermute | solution.py:13
  68.8 2.0 %collective-permute-done = bf16[2,512]{1,0:T(2,128)(2,1)S(1)} collective-permute-done((bf16[2,512]{1,0:T(2,128)(2,1)S(1)}, bf16[2,512]{1,0:T(2,128)(2,1)S(1)}, u32[]{:S(2)}, u32[]{:S(2)}) %collective-permute-start) | collective-permute-done | bytes 2080 | tf_op jit(solution)/shard_map/ppermute | solution.py:13
  70.8 2.5 %collective-permute-start.1 = (bf16[4,512]{1,0:T(4,128)(2,1)S(1)}, bf16[4,512]{1,0:T(4,128)(2,1)S(1)}, u32[]{:S(2)}, u32[]{:S(2)}) collective-permute-start(bf16[4,512]{1,0:T(4,128)(2,1)S(1)} %maximum_select_fusion.2), channel_id=1, source_target_pairs={{0,4},{2,6},{4,0},{6,2},{1,5},{3,7},{5,1},{7,3},{8,12},{10,14},{12... | collective-permute-start | bytes 12296 | tf_op jit(solution)/shard_map/ppermute | solution.py:13
  73.3 2.1 %collective-permute-done.1 = bf16[4,512]{1,0:T(4,128)(2,1)S(1)} collective-permute-done((bf16[4,512]{1,0:T(4,128)(2,1)S(1)}, bf16[4,512]{1,0:T(4,128)(2,1)S(1)}, u32[]{:S(2)}, u32[]{:S(2)}) %collective-permute-start.1) | collective-permute-done | bytes 4128 | tf_op jit(solution)/shard_map/ppermute | solution.py:13
  75.4 0.8 convolution_convert_fusion
  76.2 0.0 reduce-scatter.3.cloned.1.call-update
  76.2 0.0 reduce-scatter.5.cloned.1.call-start
  76.2 0.0 copy-done.2
  76.3 7.7 %reduce-scatter.3.cloned.1.call-done = bf16[8,256]{1,0:T(8,128)(2,1)} async-done(((bf16[8,512]{1,0:T(8,128)(2,1)}), bf16[8,256]{1,0:T(8,128)(2,1)}) %reduce-scatter.3.cloned.1.call-update) | async-done | bytes 4112 | tf_op jit(solution)/shard_map/reduce_scatter | solution.py:138
  83.9 0.7 add_convert_fusion
  84.6 14.3 %all_gather.3 = bf16[8,2048]{1,0:T(8,128)(2,1)S(1)} all-gather(bf16[8,256]{1,0:T(8,128)(2,1)S(1)} %add_convert_fusion), channel_id=1, replica_groups=mesh['dp'=4,'kv'=4,'tp'=2] {'kv','tp'}, dimensions={1}, use_global_device_ids=true | all-gather | bytes 36864 | tf_op jit(solution)/shard_map/all_gather | solution.py:145
  99.0 0.1 fusion.8
  99.1 2.7 %convolution_multiply_fusion.1 = f32[8,704]{1,0:T(8,128)S(1)} fusion(bf16[2048,704]{0,1:T(8,128)(2,1)} %param.41, bf16[8,2048]{1,0:T(8,128)(2,1)S(1)} %all_gather.3, f32[2048]{0:T(1024)S(1)} %copy-done.3, f32[8]{0:T(128)S(1)} %add_rsqrt_fusion), kind=kOutput, calls=%fused_computation.3 | convolution fusion | flops 23123456 | bytes 2947104 | tf_op jit(solution)/shard_map/dot_general | solution.py:147
  101.8 4.1 %convolution_bitcast_fusion = f32[2048,8]{0,1:T(8,128)} fusion(bf16[704,2048]{1,0:T(8,128)(2,1)S(1)} %copy-done, bf16[2048,704]{0,1:T(8,128)(2,1)} %param.42, bf16[8,2048]{1,0:T(8,128)(2,1)S(1)} %all_gather.3, f32[2048]{0:T(1024)S(1)} %copy-done.3, f32[8,704]{1,0:T(8,128)S(1)} %convolution_multiply_fusion.1, f32[8]{0:T(128)S(1)} %add_rsqrt_fusion), kind=kOutput, calls=%fused_computation | convolution fusion | flops 46225920 | bytes 5896224 | tf_op jit(solution)/shard_map/dot_general | solution.py:154
  105.9 0.0 reduce-scatter.5.cloned.1.call-update
  105.9 31.5 %reduce-scatter.5.cloned.1.call-done = f32[256,8]{0,1:T(8,128)} async-done(((f32[2048,8]{0,1:T(8,128)}), f32[256,8]{0,1:T(8,128)}) %reduce-scatter.5.cloned.1.call-update) | async-done | bytes 8208 | tf_op jit(solution)/shard_map/reduce_scatter | solution.py:153
  137.4 1.3 fusion.25
  (19 shorter events, 0.1 us)
Async XLA Ops:
  6.5 95.2 %copy-start = (bf16[704,2048]{1,0:T(8,128)(2,1)S(1)}, bf16[704,2048]{1,0:T(8,128)(2,1)}, u32[]{:S(2)}) copy-start(bf16[704,2048]{1,0:T(8,128)(2,1)} %param.43) | copy-start | bytes 8650756
  6.5 69.7 %copy-start.2 = (bf16[8,512]{1,0:T(8,128)(2,1)S(1)}, bf16[8,512]{1,0:T(8,128)(2,1)}, u32[]{:S(2)}) copy-start(bf16[8,512]{1,0:T(8,128)(2,1)} %param.22) | copy-start | bytes 24580
  6.5 68.8 %copy-start.1 = (bf16[512,512]{1,0:T(8,128)(2,1)S(1)}, bf16[512,512]{1,0:T(8,128)(2,1)}, u32[]{:S(2)}) copy-start(bf16[512,512]{1,0:T(8,128)(2,1)} %param.39) | copy-start | bytes 1572868
  6.5 92.6 %copy-start.3 = (f32[2048]{0:T(1024)S(1)}, f32[2048]{0:T(1024)}, u32[]{:S(2)}) copy-start(f32[2048]{0:T(1024)} %param.40) | copy-start | bytes 24580
  6.5 49.8 %all-reduce.8.cloned.1.call-start = ((), (), s32[]{:S(2)}) async-start(), calls=%async_computation.4 | async-start | bytes 140288
  18.6 65.4 %reduce-scatter.3.cloned.1.call-start = ((), (), s32[]{:S(2)}) async-start(), calls=%async_computation.2 | async-start | bytes 12288 | tf_op jit(solution)/shard_map/reduce_scatter | solution.py:138
  19.3 0.7 copy-start.4
  67.1 3.7 %collective-permute-start = (bf16[2,512]{1,0:T(2,128)(2,1)S(1)}, bf16[2,512]{1,0:T(2,128)(2,1)S(1)}, u32[]{:S(2)}, u32[]{:S(2)}) collective-permute-start(bf16[2,512]{1,0:T(2,128)(2,1)S(1)} %fusion.40), channel_id=1, source_target_pairs={{0,2},{2,0},{4,6},{6,4},{1,3},{3,1},{5,7},{7,5},{8,10},{10,8},{12,... | collective-permute-start | bytes 6152 | tf_op jit(solution)/shard_map/ppermute | solution.py:13
  70.8 4.6 %collective-permute-start.1 = (bf16[4,512]{1,0:T(4,128)(2,1)S(1)}, bf16[4,512]{1,0:T(4,128)(2,1)S(1)}, u32[]{:S(2)}, u32[]{:S(2)}) collective-permute-start(bf16[4,512]{1,0:T(4,128)(2,1)S(1)} %maximum_select_fusion.2), channel_id=1, source_target_pairs={{0,4},{2,6},{4,0},{6,2},{1,5},{3,7},{5,1},{7,3},{8,12},{10,14},{12... | collective-permute-start | bytes 12296 | tf_op jit(solution)/shard_map/ppermute | solution.py:13
  76.2 61.3 %reduce-scatter.5.cloned.1.call-start = ((), (), s32[]{:S(2)}) async-start(), calls=%async_computation.3 | async-start | bytes 73728 | tf_op jit(solution)/shard_map/reduce_scatter | solution.py:153
Sparse Core Ops, SparseCore 0:
  18.7 37.6 all-reduce.7
  76.3 7.5 reduce-scatter.2
  106.0 31.3 reduce-scatter.4
